TPU v7x, 256 devices: a whole 4x4x8 slice. The times are simulated.
256 devices in a mesh: fs: 32 (over z, x), tp: 8 (over y, core).
Axes of the slice: x: 4, y: 4, z: 8, core: 2. Of those that a mesh axis runs over, the one named last changes fastest.
Arguments:
- later_rows: bfloat16 [32768, 2048], P(('fs', 'tp')), may hold values from -6 to 6
- earlier_rows: bfloat16 [32768, 2048], P(('fs', 'tp')), may hold values from -6 to 6
- cotangent: bfloat16 [32768, 2048], P(('fs', 'tp')), may hold values from -24 to 24
- up_weight: bfloat16 [2048, 4096], P('fs', 'tp'), may hold values from -0.125 to 0.125
- down_weight: bfloat16 [2048, 4096], P('fs', 'tp'), may hold values from -0.09375 to 0.09375
- up_total: float32 [2048, 4096], P('fs', 'tp'), may hold values from -6 to 6
- down_total: float32 [2048, 4096], P('fs', 'tp'), may hold values from -6 to 6
Outputs:
- later_out: bfloat16 [32768, 2048], P(('fs', 'tp'))
- earlier_grad: bfloat16 [32768, 2048], P(('fs', 'tp'))
- up_updated: float32 [2048, 4096], P('fs', 'tp')
- down_updated: float32 [2048, 4096], P('fs', 'tp')
All inputs are finite; a program needn't handle non-finite values.
Results may differ from a plain program's by a relative error of at most 0.015.
Values may be sent and summed in bfloat16 or wider, within the bound.
No kernel may reach another device: no remote copies, remote signals or barrier semaphores. Data moves between devices by JAX's collectives and lax.ppermute only.
A program may use at most 128 MiB of HBM per device.

v0:
```python
import math
import jax
import jax.numpy as jnp
from jax import lax
from jax.sharding import Mesh
from jax.sharding import PartitionSpec as P

FS = ("fs_0", "fs_1")
FS_TP = ("fs_0", "fs_1", "tp")


def side_by_side(arrays, axis, dim, along):
    ends, at = ([], 0)
    for a in arrays[:-1]:
        at += a.shape[along]
        ends.append(at)
    both = jnp.concatenate(arrays, axis=along)
    return tuple(jnp.split(lax.all_gather(both, axis, axis=dim, tiled=True), ends, axis=along))


def in_blocks(x, dim, length):
    before, after = (x.shape[:dim], x.shape[dim + 1 :])
    return jnp.moveaxis(x.reshape(*before, length, -1, *after), dim, 0)


def sum_at_owner(x, axis, dim):
    length = lax.axis_size(axis)
    tiles = lax.all_to_all(in_blocks(x, dim, length), axis, 0, 0, tiled=True)
    return jnp.sum(tiles.astype(jnp.float32), axis=0)


def sum_by_axis(terms, axes):
    subtotal = terms.astype(jnp.bfloat16)
    for axis in axes:
        subtotal = lax.psum_scatter(subtotal, axis, scatter_dimension=0, tiled=True)
    return subtotal.astype(jnp.float32)


def contract_last(left, right):
    return lax.dot_general(
        left, right, (((1,), (1,)), ((), ())), preferred_element_type=jnp.float32
    )


def body(later_rows, earlier_rows, cotangent, up_weight, down_weight, up_total, down_total):
    rows_dev = later_rows.shape[0]
    total_rows = rows_dev * lax.axis_size(FS) * lax.axis_size("tp")
    factor = 1.0 / math.sqrt(total_rows)
    up_full, down_full = side_by_side((up_weight, down_weight), FS, 0, 1)

    def fetch():
        return (up_full, down_full)

    def to_owner(term):
        return sum_at_owner(term.astype(jnp.bfloat16), "tp", 0)

    def grad_owner(group, right):
        return sum_by_axis(
            lax.dot_general(
                group, right, (((0,), (0,)), ((), ())), preferred_element_type=jnp.float32
            ),
            FS,
        )

    up_whole, down_whole = fetch()
    group = lax.all_gather(later_rows, "tp", axis=0, tiled=True)
    relu_part = jnp.maximum(jnp.dot(group, up_whole, preferred_element_type=jnp.float32), 0.0)
    hidden = (relu_part * relu_part).astype(jnp.bfloat16)
    partial_value = contract_last(hidden, down_whole)
    later_out = to_owner(partial_value).astype(jnp.bfloat16)
    up_whole, down_whole = fetch()
    saved_group, cot_group = side_by_side((earlier_rows, cotangent), "tp", 0, 1)
    relu_part = jnp.maximum(jnp.dot(saved_group, up_whole, preferred_element_type=jnp.float32), 0.0)
    hidden = (relu_part * relu_part).astype(jnp.bfloat16)
    hidden_grad = jnp.dot(cot_group, down_whole, preferred_element_type=jnp.float32)
    pre_grad = (2.0 * relu_part * hidden_grad).astype(jnp.bfloat16)
    input_partial = contract_last(pre_grad, up_whole)
    earlier_grad = to_owner(input_partial).astype(jnp.bfloat16)
    down_updated = down_total + grad_owner(cot_group, hidden) * factor
    up_updated = up_total + grad_owner(saved_group, pre_grad) * factor
    earlier_grad, up_updated, down_updated = (earlier_grad, up_updated, down_updated)
    return (later_out, earlier_grad, up_updated, down_updated)


def solution(mesh):
    finer = Mesh(mesh.devices.reshape(8, 4, mesh.shape["tp"]), ("fs_0", "fs_1", "tp"))
    placed = (
        P(FS_TP, None),
        P(FS_TP, None),
        P(FS_TP, None),
        P(FS, "tp"),
        P(FS, "tp"),
        P(FS, "tp"),
        P(FS, "tp"),
    )
    return jax.shard_map(
        body,
        mesh=finer,
        in_specs=placed,
        out_specs=(P(FS_TP, None), P(FS_TP, None), P(FS, "tp"), P(FS, "tp")),
        check_vma=False,
    )
```

profile of v0, /device:TPU:8, one launch (start us, length us, event | category | flops | bytes accessed | tf_op | source)
XLA Modules:
  0.0 330.6 jit_solution(11753121503092980763)
XLA Ops:
  7.2 1.5 pad_maximum_fusion.1
  8.8 0.0 all-gather.8.cloned.1.call-start
  8.8 2.3 pad_maximum_fusion
  11.2 0.7 all-gather.6.cloned.1.call-update
  11.9 83.9 %all-gather.4.cloned.1.call-done = bf16[2048,1024]{1,0:T(8,128)(2,1)} async-done(((bf16[64,1024]{1,0:T(8,128)(2,1)}), bf16[2048,1024]{1,0:T(8,128)(2,1)}) %all-gather.4.cloned.1.call-update) | async-done | bytes 4194320 | tf_op jit(solution)/shard_map/all_gather | solution.py:18
  95.8 50.1 %all-gather.8.cloned.1.call-done = bf16[1024,4096]{1,0:T(8,128)(2,1)} async-done(((bf16[128,4096]{1,0:T(8,128)(2,1)}), bf16[1024,4096]{1,0:T(8,128)(2,1)}) %all-gather.8.cloned.1.call-update) | async-done | bytes 8388624 | tf_op jit(solution)/shard_map/all_gather | solution.py:18
  145.9 5.3 %fusion.6 = f32[1024,512]{1,0:T(8,128)S(1)} fusion(bf16[1024,4096]{1,0:T(8,128)(2,1)} %all-gather.8.cloned.1.call-done, bf16[2048,1024]{1,0:T(8,128)(2,1)} %all-gather.4.cloned.1.call-done), kind=kOutput, calls=%fused_computation.8 | convolution fusion | flops 2147483648 | bytes 8388608 | tf_op jit(solution)/shard_map/dot_general | solution.py:73
  151.2 3.7 %fusion.11 = bf16[2048,512]{1,0:T(8,128)(2,1)} fusion(bf16[1024,4096]{1,0:T(8,128)(2,1)S(1)} %copy-done.2, f32[1024,512]{1,0:T(8,128)S(1)} %fusion.6), kind=kOutput, calls=%fused_computation.11 | convolution fusion | flops 2150105088 | bytes 8388608 | tf_op jit(solution)/shard_map/dot_general | solution.py:59
  155.0 27.4 %all-gather.6.cloned.1.call-done = bf16[1024,2048]{1,0:T(8,128)(2,1)} async-done(((bf16[128,2048]{1,0:T(8,128)(2,1)}), bf16[1024,2048]{1,0:T(8,128)(2,1)}) %all-gather.6.cloned.1.call-update) | async-done | bytes 4194320 | tf_op jit(solution)/shard_map/all_gather | solution.py:66
  182.4 10.0 %convolution_convert_fusion.1 = bf16[1024,2048]{1,0:T(8,128)(2,1)} fusion(bf16[2048,1024]{1,0:T(8,128)(2,1)} %all-gather.4.cloned.1.call-done, bf16[1024,2048]{1,0:T(8,128)(2,1)} %all-gather.6.cloned.1.call-done), kind=kOutput, calls=%fused_computation.1 | convolution fusion | flops 4298637312 | bytes 12582912 | tf_op jit(solution)/shard_map/dot_general | solution.py:40
  192.4 6.0 %all-to-all-start = ((bf16[8,128,2048]{2,1,0:T(8,128)(2,1)}), bf16[8,128,2048]{2,1,0:T(8,128)(2,1)}, u32[]{:S(2)}, u32[]{:S(2)}) async-start(bf16[8,128,2048]{2,1,0:T(8,128)(2,1)} %bitcast.6), calls=%async_computation | async-start | bytes 8388608 | tf_op jit(solution)/shard_map/all_to_all | solution.py:28
  198.4 5.2 %multiply_convert_fusion.1 = bf16[1024,512]{1,0:T(8,128)(2,1)S(1)} fusion(f32[1024,512]{1,0:T(8,128)S(1)} %fusion.6, bf16[2048,1024]{1,0:T(8,128)(2,1)} %all-gather.4.cloned.1.call-done, bf16[1024,4096]{1,0:T(8,128)(2,1)} %all-gather.8.cloned.1.call-done), kind=kOutput, calls=%fused_computation.13 | convolution fusion | flops 2149580800 | bytes 9437184 | tf_op jit(solution)/shard_map/dot_general | solution.py:75
  203.6 6.0 %fusion.8 = bf16[2048,512]{1,0:T(8,128)(2,1)} fusion(bf16[1024,512]{1,0:T(8,128)(2,1)S(1)} %multiply_convert_fusion.1, bf16[1024,4096]{1,0:T(8,128)(2,1)} %all-gather.8.cloned.1.call-done), kind=kOutput, calls=%fused_computation.10 | convolution fusion | flops 2148532224 | bytes 7340032 | tf_op jit(solution)/shard_map/dot_general | solution.py:59
  209.6 5.9 %convolution_convert_fusion = bf16[1024,2048]{1,0:T(8,128)(2,1)} fusion(bf16[1024,512]{1,0:T(8,128)(2,1)S(1)} %multiply_convert_fusion.1, bf16[2048,1024]{1,0:T(8,128)(2,1)} %all-gather.4.cloned.1.call-done), kind=kOutput, calls=%fused_computation | convolution fusion | flops 2149580800 | bytes 7340032 | tf_op jit(solution)/shard_map/dot_general | solution.py:40
  215.5 31.2 %all-to-all-done = bf16[8,128,2048]{2,1,0:T(8,128)(2,1)} async-done(((bf16[8,128,2048]{2,1,0:T(8,128)(2,1)}), bf16[8,128,2048]{2,1,0:T(8,128)(2,1)}, u32[]{:S(2)}, u32[]{:S(2)}) %all-to-all-start) | async-done | bytes 4194336 | tf_op jit(solution)/shard_map/all_to_all | solution.py:28
  246.7 5.9 %all-to-all-start.1 = ((bf16[8,128,2048]{2,1,0:T(8,128)(2,1)}), bf16[8,128,2048]{2,1,0:T(8,128)(2,1)}, u32[]{:S(2)}, u32[]{:S(2)}) async-start(bf16[8,128,2048]{2,1,0:T(8,128)(2,1)} %bitcast.5), calls=%async_computation.1 | async-start | bytes 8388608 | tf_op jit(solution)/shard_map/all_to_all | solution.py:28
  252.6 0.6 reduce-scatter.11.cloned.1.call-update
  253.2 18.8 %reduce-scatter.5.cloned.1.call-done = bf16[256,512]{1,0:T(8,128)(2,1)} async-done(((bf16[2048,512]{1,0:T(8,128)(2,1)}), bf16[256,512]{1,0:T(8,128)(2,1)}) %reduce-scatter.5.cloned.1.call-update) | async-done | bytes 262160 | tf_op jit(solution)/shard_map/reduce_scatter | solution.py:35
  272.0 3.9 %reduce_sum.24 = bf16[128,2048]{1,0:T(8,128)(2,1)} reduce(bf16[8,128,2048]{2,1,0:T(8,128)(2,1)} %all-to-all-done, bf16[]{:T(256)} %constant.3.clone.1), dimensions={0}, to_apply=%region_0.0 | reduce | flops 1835008 | bytes 4718594 | tf_op jit(solution)/shard_map/reduce_sum | solution.py:29
  275.9 25.0 %all-to-all-done.1 = bf16[8,128,2048]{2,1,0:T(8,128)(2,1)} async-done(((bf16[8,128,2048]{2,1,0:T(8,128)(2,1)}), bf16[8,128,2048]{2,1,0:T(8,128)(2,1)}, u32[]{:S(2)}, u32[]{:S(2)}) %all-to-all-start.1) | async-done | bytes 4194336 | tf_op jit(solution)/shard_map/all_to_all | solution.py:28
  300.9 3.8 %reduce_sum.25 = bf16[128,2048]{1,0:T(8,128)(2,1)} reduce(bf16[8,128,2048]{2,1,0:T(8,128)(2,1)} %all-to-all-done.1, bf16[]{:T(256)} %constant.3.clone.1), dimensions={0}, to_apply=%region_1.0 | reduce | flops 1835008 | bytes 4718594 | tf_op jit(solution)/shard_map/reduce_sum | solution.py:29
  304.8 1.5 multiply_add_fusion
  306.3 16.0 %reduce-scatter.7.cloned.1.call-done = bf16[64,512]{1,0:T(8,128)(2,1)} async-done(((bf16[256,512]{1,0:T(8,128)(2,1)}), bf16[64,512]{1,0:T(8,128)(2,1)}) %reduce-scatter.7.cloned.1.call-update) | async-done | bytes 65552 | tf_op jit(solution)/shard_map/reduce_scatter | solution.py:35
  322.3 1.5 multiply_add_fusion.1
  (19 shorter events, 0.3 us)
Async XLA Ops:
  7.2 88.6 %all-gather.4.cloned.1.call-start = ((), (), s32[]{:S(2)}) async-start(), calls=%async_computation.6 | async-start | bytes 4325376 | tf_op jit(solution)/shard_map/all_gather | solution.py:18
  8.8 137.1 %all-gather.8.cloned.1.call-start = ((), (), s32[]{:S(2)}) async-start(), calls=%async_computation.8 | async-start | bytes 9437184 | tf_op jit(solution)/shard_map/all_gather | solution.py:18
  11.1 171.2 %all-gather.6.cloned.1.call-start = ((), (), s32[]{:S(2)}) async-start(), calls=%async_computation.7 | async-start | bytes 4718592 | tf_op jit(solution)/shard_map/all_gather | solution.py:66
  11.9 240.7 %reduce-scatter.9.cloned.1.call-start = ((), (), s32[]{:S(2)}) async-start(), calls=%async_computation.11 | async-start | bytes 2359296 | tf_op jit(solution)/shard_map/reduce_scatter | solution.py:35
  145.9 5.3 %copy-start.2 = (bf16[1024,4096]{1,0:T(8,128)(2,1)S(1)}, bf16[1024,4096]{1,0:T(8,128)(2,1)}, u32[]{:S(2)}) copy-start(bf16[1024,4096]{1,0:T(8,128)(2,1)} %all-gather.8.cloned.1.call-done) | copy-start | bytes 25165828
  192.4 54.3 %all-to-all-start = ((bf16[8,128,2048]{2,1,0:T(8,128)(2,1)}), bf16[8,128,2048]{2,1,0:T(8,128)(2,1)}, u32[]{:S(2)}, u32[]{:S(2)}) async-start(bf16[8,128,2048]{2,1,0:T(8,128)(2,1)} %bitcast.6), calls=%async_computation | async-start | bytes 8388608 | tf_op jit(solution)/shard_map/all_to_all | solution.py:28
  198.4 73.6 %reduce-scatter.5.cloned.1.call-start = ((), (), s32[]{:S(2)}) async-start(), calls=%async_computation.9 | async-start | bytes 2359296 | tf_op jit(solution)/shard_map/reduce_scatter | solution.py:35
  246.7 54.2 %all-to-all-start.1 = ((bf16[8,128,2048]{2,1,0:T(8,128)(2,1)}), bf16[8,128,2048]{2,1,0:T(8,128)(2,1)}, u32[]{:S(2)}, u32[]{:S(2)}) async-start(bf16[8,128,2048]{2,1,0:T(8,128)(2,1)} %bitcast.5), calls=%async_computation.1 | async-start | bytes 8388608 | tf_op jit(solution)/shard_map/all_to_all | solution.py:28
  252.6 52.2 %reduce-scatter.11.cloned.1.call-start = ((), (), s32[]{:S(2)}) async-start(), calls=%async_computation.12 | async-start | bytes 327680 | tf_op jit(solution)/shard_map/reduce_scatter | solution.py:35
  253.2 69.1 %reduce-scatter.7.cloned.1.call-start = ((), (), s32[]{:S(2)}) async-start(), calls=%async_computation.10 | async-start | bytes 327680 | tf_op jit(solution)/shard_map/reduce_scatter | solution.py:35
  272.0 32.8 %copy-start = (f32[64,512]{1,0:T(8,128)S(1)}, f32[64,512]{1,0:T(8,128)}, u32[]{:S(2)}) copy-start(f32[64,512]{1,0:T(8,128)} %param.13) | copy-start | bytes 393220
  272.0 50.3 %copy-start.1 = (f32[64,512]{1,0:T(8,128)S(1)}, f32[64,512]{1,0:T(8,128)}, u32[]{:S(2)}) copy-start(f32[64,512]{1,0:T(8,128)} %param.12) | copy-start | bytes 393220
Sparse Core Ops, SparseCore 0:
  11.1 84.6 all-gather.3
  97.6 48.1 all-gather.7
  147.8 34.5 all-gather.5
  184.8 43.4 reduce-scatter.8
  230.7 41.2 reduce-scatter.4
  274.3 22.1 reduce-scatter.10
  299.1 23.1 reduce-scatter.6
where the time goes:
time: 331 us
  waiting for transfers between devices  254 us (77%)
  matrix products  36.1 us (11%)
  other arithmetic  14.6 us (4%)
  between operations  14.2 us (4%)
  starting transfers between devices  12.1 us (4%)
    all_gather x2, waiting for transfers between devices, side_by_side(): lax.all_gather(both, axis, axis=dim, tiled=True)  134 us
    all_to_all x2, waiting for transfers between devices, sum_at_owner(): tiles = lax.all_to_all(in_blocks(x, dim, length), axis, 0, 0, tiled=True)  56.2 us
    reduce_scatter x4, waiting for transfers between devices, sum_by_axis(): subtotal = lax.psum_scatter(subtotal, axis, scatter_dimension=0, tiled=True)  34.8 us
    all_gather x1, waiting for transfers between devices, body(): group = lax.all_gather(later_rows, 'tp', axis=0, tiled=True)  27.4 us
    dot_general x2, matrix products, contract_last(): lax.dot_general(left, right, (((1,), (1,)), ((), ())), preferred_element_...  15.9 us
    all_to_all x2, starting transfers between devices, sum_at_owner(): tiles = lax.all_to_all(in_blocks(x, dim, length), axis, 0, 0, tiled=True)  11.9 us
    dot_general x2, matrix products, grad_owner(): lax.dot_general(group, right, (((0,), (0,)), ((), ())), preferred_element...  9.68 us
    reduce_sum x2, other arithmetic, sum_at_owner(): return jnp.sum(tiles.astype(jnp.float32), axis=0)  7.73 us
  transfers between devices with their start and end apart: 9, of which 7 were waited for; matrix products, arithmetic and copies ran while one was open for 14% of the time, Pallas kernels for 0%

commit v1 on v0

--- a/solution.py
+++ b/solution.py
@@ -7,6 +7,23 @@
 
 FS = ("fs_0", "fs_1")
 FS_TP = ("fs_0", "fs_1", "tp")
+
+
+def joined_along(tiles, dim):
+    shape = list(tiles.shape[1:])
+    shape[dim] *= tiles.shape[0]
+    return jnp.moveaxis(tiles, 0, dim).reshape(shape)
+
+
+def grow_blocks(x, axis):
+    size, place = (lax.axis_size(axis), lax.axis_index(axis))
+    blocks, bit = (x[None], 1)
+    while bit < size:
+        theirs = lax.ppermute(blocks, axis, [(i, i ^ bit) for i in range(size)])
+        low = place & bit == 0
+        blocks = jnp.concatenate([jnp.where(low, blocks, theirs), jnp.where(low, theirs, blocks)])
+        bit *= 2
+    return blocks
 
 
 def side_by_side(arrays, axis, dim, along):
@@ -63,7 +80,7 @@
         )
 
     up_whole, down_whole = fetch()
-    group = lax.all_gather(later_rows, "tp", axis=0, tiled=True)
+    group = joined_along(grow_blocks(later_rows, "tp"), 0)
     relu_part = jnp.maximum(jnp.dot(group, up_whole, preferred_element_type=jnp.float32), 0.0)
     hidden = (relu_part * relu_part).astype(jnp.bfloat16)
     partial_value = contract_last(hidden, down_whole)

time: 331 us -> 303 us (0.915)
  waiting for transfers between devices: 254 us -> 212 us
  other arithmetic: 14.6 us -> 21.8 us
  starting transfers between devices: 12.1 us -> 16.2 us
    all_gather x2, waiting for transfers between devices: 134 us -> 102 us  [side_by_side(): lax.all_gather(both, axis, axis=dim, tiled=True)]
    all_gather x1 -> x0, waiting for transfers between devices: 27.4 us -> none  [body(): group = lax.all_gather(later_rows, 'tp', axis=0, tiled=True)]
    ppermute x0 -> x3, waiting for transfers between devices: none -> 25.5 us  [grow_blocks(): theirs = lax.ppermute(blocks, axis, [(i, i ^ bit) for i in range(size)])]
    reduce_scatter x4, waiting for transfers between devices: 34.8 us -> 21.8 us  [sum_by_axis(): subtotal = lax.psum_scatter(subtotal, axis, scatter_dimension=0, tiled=True)]
    all_to_all x2, waiting for transfers between devices: 56.2 us -> 62.4 us  [sum_at_owner(): tiles = lax.all_to_all(in_blocks(x, dim, length), axis, 0, 0, tiled=True)]
    ppermute x0 -> x3, starting transfers between devices: none -> 4.21 us  [grow_blocks(): theirs = lax.ppermute(blocks, axis, [(i, i ^ bit) for i in range(size)])]
    concatenate x0 -> x3, other arithmetic: none -> 3.94 us  [grow_blocks(): jnp.concatenate([jnp.where(low, blocks, theirs), jnp.where(low, theirs, b...]
  transfers between devices with their start and end apart: 9 -> 11, of which waited for: 7 -> 8; matrix products, arithmetic and copies ran while one was open for 14% -> 18% of each run, Pallas kernels for 0% -> 0%
where the time goes in v1:
time: 303 us; the launch traced here: 302 us
  waiting for transfers between devices  212 us (70%)
  matrix products  36.2 us (12%)
  other arithmetic  21.8 us (7%)
  starting transfers between devices  16.2 us (5%)
  between operations  14.2 us (5%)
    all_gather x2, waiting for transfers between devices, side_by_side(): lax.all_gather(both, axis, axis=dim, tiled=True)  102 us
    all_to_all x2, waiting for transfers between devices, sum_at_owner(): tiles = lax.all_to_all(in_blocks(x, dim, length), axis, 0, 0, tiled=True)  62.4 us
    ppermute x3, waiting for transfers between devices, grow_blocks(): theirs = lax.ppermute(blocks, axis, [(i, i ^ bit) for i in range(size)])  25.5 us
    reduce_scatter x4, waiting for transfers between devices, sum_by_axis(): subtotal = lax.psum_scatter(subtotal, axis, scatter_dimension=0, tiled=True)  21.8 us
    dot_general x2, matrix products, contract_last(): lax.dot_general(left, right, (((1,), (1,)), ((), ())), preferred_element_...  15.9 us
    all_to_all x2, starting transfers between devices, sum_at_owner(): tiles = lax.all_to_all(in_blocks(x, dim, length), axis, 0, 0, tiled=True)  11.8 us
    dot_general x2, matrix products, grad_owner(): lax.dot_general(group, right, (((0,), (0,)), ((), ())), preferred_element...  9.68 us
    reduce_sum x2, other arithmetic, sum_at_owner(): return jnp.sum(tiles.astype(jnp.float32), axis=0)  7.7 us
  transfers between devices with their start and end apart: 11, of which 8 were waited for; matrix products, arithmetic and copies ran while one was open for 18% of the time, Pallas kernels for 0%

profile of v1, /device:TPU:8, one launch (start us, length us, event | category | flops | bytes accessed | tf_op | source)
XLA Modules:
  0.0 302.1 jit_solution(2056050130769653822)
XLA Ops:
  7.2 1.6 pad_maximum_fusion.4
  8.9 2.3 pad_maximum_fusion.3
  11.4 1.9 collective-permute-done
  13.4 2.2 collective-permute-start.1
  15.7 23.6 %collective-permute-done.1 = bf16[2,128,2048]{2,1,0:T(8,128)(2,1)} collective-permute-done((bf16[2,128,2048]{2,1,0:T(8,128)(2,1)S(1)}, bf16[2,128,2048]{2,1,0:T(8,128)(2,1)}, u32[]{:S(2)}, u32[]{:S(2)}) %collective-permute-start.1) | collective-permute-done | bytes 1048608 | tf_op jit(solution)/shard_map/ppermute | solution.py:22
  42.1 1.9 collective-permute-start.2
  44.0 51.8 %all-gather.3.cloned.1.call-done = bf16[2048,1024]{1,0:T(8,128)(2,1)} async-done(((bf16[64,1024]{1,0:T(8,128)(2,1)}), bf16[2048,1024]{1,0:T(8,128)(2,1)}) %all-gather.3.cloned.1.call-update) | async-done | bytes 4194320 | tf_op jit(solution)/shard_map/all_gather | solution.py:35
  95.8 50.1 %all-gather.5.cloned.1.call-done = bf16[1024,4096]{1,0:T(8,128)(2,1)} async-done(((bf16[128,4096]{1,0:T(8,128)(2,1)}), bf16[1024,4096]{1,0:T(8,128)(2,1)}) %all-gather.5.cloned.1.call-update) | async-done | bytes 8388624 | tf_op jit(solution)/shard_map/all_gather | solution.py:35
  145.9 5.3 %fusion.6 = f32[1024,512]{1,0:T(8,128)S(1)} fusion(bf16[1024,4096]{1,0:T(8,128)(2,1)} %all-gather.5.cloned.1.call-done, bf16[2048,1024]{1,0:T(8,128)(2,1)} %all-gather.3.cloned.1.call-done), kind=kOutput, calls=%fused_computation.9 | convolution fusion | flops 2147483648 | bytes 8388608 | tf_op jit(solution)/shard_map/dot_general | solution.py:90
  152.6 3.7 %fusion.11 = bf16[2048,512]{1,0:T(8,128)(2,1)} fusion(bf16[1024,4096]{1,0:T(8,128)(2,1)S(1)} %copy-done.3, f32[1024,512]{1,0:T(8,128)S(1)} %fusion.6), kind=kOutput, calls=%fused_computation.12 | convolution fusion | flops 2150105088 | bytes 8388608 | tf_op jit(solution)/shard_map/dot_general | solution.py:76
  156.3 1.9 broadcast_select_fusion.1
  158.2 2.3 pad_maximum_fusion
  160.6 9.9 %convolution_convert_fusion.1 = bf16[1024,2048]{1,0:T(8,128)(2,1)} fusion(bf16[2048,1024]{1,0:T(8,128)(2,1)} %all-gather.3.cloned.1.call-done, bf16[1024,2048]{1,0:T(8,128)(2,1)} %bitcast.11), kind=kOutput, calls=%fused_computation.2 | convolution fusion | flops 4298637312 | bytes 12582912 | tf_op jit(solution)/shard_map/dot_general | solution.py:57
  170.5 5.9 %all-to-all-start = ((bf16[8,128,2048]{2,1,0:T(8,128)(2,1)}), bf16[8,128,2048]{2,1,0:T(8,128)(2,1)}, u32[]{:S(2)}, u32[]{:S(2)}) async-start(bf16[8,128,2048]{2,1,0:T(8,128)(2,1)} %bitcast.10), calls=%async_computation | async-start | bytes 8388608 | tf_op jit(solution)/shard_map/all_to_all | solution.py:45
  176.4 5.2 %multiply_convert_fusion.1 = bf16[1024,512]{1,0:T(8,128)(2,1)S(1)} fusion(f32[1024,512]{1,0:T(8,128)S(1)} %copy-done.5, bf16[2048,1024]{1,0:T(8,128)(2,1)} %all-gather.3.cloned.1.call-done, bf16[1024,4096]{1,0:T(8,128)(2,1)} %all-gather.5.cloned.1.call-done), kind=kOutput, calls=%fused_computation.15 | convolution fusion | flops 2149580800 | bytes 9437184 | tf_op jit(solution)/shard_map/dot_general | solution.py:92
  181.7 6.0 %fusion.8 = bf16[2048,512]{1,0:T(8,128)(2,1)} fusion(bf16[1024,512]{1,0:T(8,128)(2,1)S(1)} %multiply_convert_fusion.1, bf16[1024,4096]{1,0:T(8,128)(2,1)} %all-gather.5.cloned.1.call-done), kind=kOutput, calls=%fused_computation.11 | convolution fusion | flops 2148532224 | bytes 7340032 | tf_op jit(solution)/shard_map/dot_general | solution.py:76
  187.7 6.0 %convolution_convert_fusion = bf16[1024,2048]{1,0:T(8,128)(2,1)} fusion(bf16[1024,512]{1,0:T(8,128)(2,1)S(1)} %multiply_convert_fusion.1, bf16[2048,1024]{1,0:T(8,128)(2,1)} %all-gather.3.cloned.1.call-done), kind=kOutput, calls=%fused_computation.1 | convolution fusion | flops 2149580800 | bytes 7340032 | tf_op jit(solution)/shard_map/dot_general | solution.py:57
  193.7 31.0 %all-to-all-done = bf16[8,128,2048]{2,1,0:T(8,128)(2,1)} async-done(((bf16[8,128,2048]{2,1,0:T(8,128)(2,1)}), bf16[8,128,2048]{2,1,0:T(8,128)(2,1)}, u32[]{:S(2)}, u32[]{:S(2)}) %all-to-all-start) | async-done | bytes 4194336 | tf_op jit(solution)/shard_map/all_to_all | solution.py:45
  224.8 5.9 %all-to-all-start.1 = ((bf16[8,128,2048]{2,1,0:T(8,128)(2,1)}), bf16[8,128,2048]{2,1,0:T(8,128)(2,1)}, u32[]{:S(2)}, u32[]{:S(2)}) async-start(bf16[8,128,2048]{2,1,0:T(8,128)(2,1)} %bitcast.9), calls=%async_computation.1 | async-start | bytes 8388608 | tf_op jit(solution)/shard_map/all_to_all | solution.py:45
  231.3 12.4 %reduce-scatter.5.cloned.1.call-done = bf16[256,512]{1,0:T(8,128)(2,1)} async-done(((bf16[2048,512]{1,0:T(8,128)(2,1)}), bf16[256,512]{1,0:T(8,128)(2,1)}) %reduce-scatter.5.cloned.1.call-update) | async-done | bytes 262160 | tf_op jit(solution)/shard_map/reduce_scatter | solution.py:52
  243.7 3.8 %reduce_sum.24 = bf16[128,2048]{1,0:T(8,128)(2,1)} reduce(bf16[8,128,2048]{2,1,0:T(8,128)(2,1)} %all-to-all-done, bf16[]{:T(256)} %constant.8.clone.1), dimensions={0}, to_apply=%region_0.1 | reduce | flops 1835008 | bytes 4718594 | tf_op jit(solution)/shard_map/reduce_sum | solution.py:46
  247.6 31.4 %all-to-all-done.1 = bf16[8,128,2048]{2,1,0:T(8,128)(2,1)} async-done(((bf16[8,128,2048]{2,1,0:T(8,128)(2,1)}), bf16[8,128,2048]{2,1,0:T(8,128)(2,1)}, u32[]{:S(2)}, u32[]{:S(2)}) %all-to-all-start.1) | async-done | bytes 4194336 | tf_op jit(solution)/shard_map/all_to_all | solution.py:45
  279.0 3.8 %reduce_sum.25 = bf16[128,2048]{1,0:T(8,128)(2,1)} reduce(bf16[8,128,2048]{2,1,0:T(8,128)(2,1)} %all-to-all-done.1, bf16[]{:T(256)} %constant.8.clone.1), dimensions={0}, to_apply=%region_1.2 | reduce | flops 1835008 | bytes 4718594 | tf_op jit(solution)/shard_map/reduce_sum | solution.py:46
  284.3 9.4 %reduce-scatter.7.cloned.1.call-done = bf16[64,512]{1,0:T(8,128)(2,1)} async-done(((bf16[256,512]{1,0:T(8,128)(2,1)}), bf16[64,512]{1,0:T(8,128)(2,1)}) %reduce-scatter.7.cloned.1.call-update) | async-done | bytes 65552 | tf_op jit(solution)/shard_map/reduce_scatter | solution.py:52
  (34 shorter events, 8.4 us)
Async XLA Ops:
  7.2 4.1 %copy-start = (bf16[128,2048]{1,0:T(8,128)(2,1)S(1)}, bf16[128,2048]{1,0:T(8,128)(2,1)}, u32[]{:S(2)}) copy-start(bf16[128,2048]{1,0:T(8,128)(2,1)} %param.7) | copy-start | bytes 1572868
  7.2 88.6 %all-gather.3.cloned.1.call-start = ((), (), s32[]{:S(2)}) async-start(), calls=%async_computation.6 | async-start | bytes 4325376 | tf_op jit(solution)/shard_map/all_gather | solution.py:35
  8.8 137.1 %all-gather.5.cloned.1.call-start = ((), (), s32[]{:S(2)}) async-start(), calls=%async_computation.7 | async-start | bytes 9437184 | tf_op jit(solution)/shard_map/all_gather | solution.py:35
  11.2 219.5 %reduce-scatter.9.cloned.1.call-start = ((), (), s32[]{:S(2)}) async-start(), calls=%async_computation.10 | async-start | bytes 2359296 | tf_op jit(solution)/shard_map/reduce_scatter | solution.py:52
  11.3 2.0 collective-permute-start
  13.4 25.8 %collective-permute-start.1 = (bf16[2,128,2048]{2,1,0:T(8,128)(2,1)S(1)}, bf16[2,128,2048]{2,1,0:T(8,128)(2,1)}, u32[]{:S(2)}, u32[]{:S(2)}) collective-permute-start(bf16[2,128,2048]{2,1,0:T(8,128)(2,1)S(1)} %pad_maximum_fusion.2), channel_id=1, source_target_pairs={{0,2},{1,3},{2,0},{3,1},{4,6},{5,7},{6,4},{7,5},{8,10},{9,11},{10,... | collective-permute-start | bytes 3145736 | tf_op jit(solution)/shard_map/ppermute | solution.py:22
  42.1 114.2 %collective-permute-start.2 = (bf16[4,128,2048]{2,1,0:T(8,128)(2,1)}, bf16[4,128,2048]{2,1,0:T(8,128)(2,1)}, u32[]{:S(2)}, u32[]{:S(2)}) collective-permute-start(bf16[4,128,2048]{2,1,0:T(8,128)(2,1)} %pad_maximum_fusion.1), channel_id=1, source_target_pairs={{0,4},{1,5},{2,6},{3,7},{4,0},{5,1},{6,2},{7,3},{8,12},{9,13},{10,... | collective-permute-start | bytes 6291464 | tf_op jit(solution)/shard_map/ppermute | solution.py:22
  145.9 6.7 %copy-start.3 = (bf16[1024,4096]{1,0:T(8,128)(2,1)S(1)}, bf16[1024,4096]{1,0:T(8,128)(2,1)}, u32[]{:S(2)}) copy-start(bf16[1024,4096]{1,0:T(8,128)(2,1)} %all-gather.5.cloned.1.call-done) | copy-start | bytes 25165828
  151.2 1.4 copy-start.4
  170.5 6.0 %copy-start.5 = (f32[1024,512]{1,0:T(8,128)S(1)}, f32[1024,512]{1,0:T(8,128)}, u32[]{:S(2)}) copy-start(f32[1024,512]{1,0:T(8,128)} %copy-done.4) | copy-start | bytes 6291460
  170.5 54.3 %all-to-all-start = ((bf16[8,128,2048]{2,1,0:T(8,128)(2,1)}), bf16[8,128,2048]{2,1,0:T(8,128)(2,1)}, u32[]{:S(2)}, u32[]{:S(2)}) async-start(bf16[8,128,2048]{2,1,0:T(8,128)(2,1)} %bitcast.10), calls=%async_computation | async-start | bytes 8388608 | tf_op jit(solution)/shard_map/all_to_all | solution.py:45
  176.4 67.2 %reduce-scatter.5.cloned.1.call-start = ((), (), s32[]{:S(2)}) async-start(), calls=%async_computation.8 | async-start | bytes 2359296 | tf_op jit(solution)/shard_map/reduce_scatter | solution.py:52
  224.8 54.2 %all-to-all-start.1 = ((bf16[8,128,2048]{2,1,0:T(8,128)(2,1)}), bf16[8,128,2048]{2,1,0:T(8,128)(2,1)}, u32[]{:S(2)}, u32[]{:S(2)}) async-start(bf16[8,128,2048]{2,1,0:T(8,128)(2,1)} %bitcast.9), calls=%async_computation.1 | async-start | bytes 8388608 | tf_op jit(solution)/shard_map/all_to_all | solution.py:45
  230.6 52.2 %reduce-scatter.11.cloned.1.call-start = ((), (), s32[]{:S(2)}) async-start(), calls=%async_computation.11 | async-start | bytes 327680 | tf_op jit(solution)/shard_map/reduce_scatter | solution.py:52
  231.2 62.5 %reduce-scatter.7.cloned.1.call-start = ((), (), s32[]{:S(2)}) async-start(), calls=%async_computation.9 | async-start | bytes 327680 | tf_op jit(solution)/shard_map/reduce_scatter | solution.py:52
  247.6 35.3 %copy-start.1 = (f32[64,512]{1,0:T(8,128)S(1)}, f32[64,512]{1,0:T(8,128)}, u32[]{:S(2)}) copy-start(f32[64,512]{1,0:T(8,128)} %param.13) | copy-start | bytes 393220
  247.6 46.2 %copy-start.2 = (f32[64,512]{1,0:T(8,128)S(1)}, f32[64,512]{1,0:T(8,128)}, u32[]{:S(2)}) copy-start(f32[64,512]{1,0:T(8,128)} %param.12) | copy-start | bytes 393220
Sparse Core Ops, SparseCore 0:
  11.1 84.6 all-gather.2
  97.6 48.1 all-gather.4
  156.4 43.7 reduce-scatter.8
  202.6 41.0 reduce-scatter.4
  246.0 22.0 reduce-scatter.10
  270.5 23.1 reduce-scatter.6
